TPU v7x, 32 devices: a whole 2x2x4 slice. The times are simulated.
32 devices in a mesh: kv: 8 (over z, x), tp: 4 (over y, core).
Axes of the slice: x: 2, y: 2, z: 4, core: 2. Of those that a mesh axis runs over, the one named last changes fastest.
Arguments:
- tokens: bfloat16 [64, 12, 4096], P(None, None, 'kv'), may hold values from -6 to 6
- parents: int32 [64, 12], P('kv'), may hold values from -1 to 10, as said below
- accepted: int32 [64], P('kv'), may hold values from 0 to 6
- state: float32 [64, 64, 64, 128], P('kv', 'tp'), may hold values from -4 to 4
- conv_x: bfloat16 [64, 3, 4096], P('kv', None, 'tp'), may hold values from -6 to 6
- conv_b: bfloat16 [64, 3, 2048], P('kv', None, 'tp'), may hold values from -6 to 6
- conv_c: bfloat16 [64, 3, 2048], P('kv', None, 'tp'), may hold values from -6 to 6
- path_x: bfloat16 [64, 6, 4096], P('kv', None, 'tp'), may hold values from -6 to 6
- path_b: bfloat16 [64, 6, 2048], P('kv', None, 'tp'), may hold values from -6 to 6
- path_c: bfloat16 [64, 6, 2048], P('kv', None, 'tp'), may hold values from -6 to 6
- path_dt: bfloat16 [64, 6, 64], P('kv', None, 'tp'), may hold values from -6 to 6
- gain_in: float32 [4096], replicated, may hold values from 0.1 to 1.9
- w_x: bfloat16 [4096, 4096], P('kv', 'tp'), may hold values from -0.09375 to 0.09375
- w_z: bfloat16 [4096, 4096], P('kv', 'tp'), may hold values from -0.09375 to 0.09375
- w_b: bfloat16 [4096, 2048], P('kv', 'tp'), may hold values from -0.09375 to 0.09375
- w_c: bfloat16 [4096, 2048], P('kv', 'tp'), may hold values from -0.09375 to 0.09375
- w_dt: bfloat16 [4096, 64], replicated, may hold values from -0.09375 to 0.09375
- dt_bias: float32 [64], P('tp'), may hold values from -2 to 1
- a_log: float32 [64], P('tp'), may hold values from -3 to 1.5
- d_skip: float32 [64], P('tp'), may hold values from 0.5 to 1.5
- conv_wx: bfloat16 [4, 4096], P(None, 'tp'), may hold values from -3 to 3
- conv_wb: bfloat16 [4, 2048], P(None, 'tp'), may hold values from -3 to 3
- conv_wc: bfloat16 [4, 2048], P(None, 'tp'), may hold values from -3 to 3
- gain_out: float32 [4096], P('tp'), may hold values from 0.1 to 1.9
- w_out: bfloat16 [4096, 4096], P('tp', 'kv'), may hold values from -0.09375 to 0.09375
Outputs:
- mixed: bfloat16 [64, 12, 4096], P('kv', None, 'tp')
- new_state: float32 [64, 64, 64, 128], P('kv', 'tp')
Inputs may be any that keep to these rules, and one draw needn't show every extreme that they name: `parents`: each proposal's parent is -1 or an earlier proposal of the same sequence; the first proposal's parent is -1.
All inputs are finite; a program needn't handle non-finite values.
Results may differ from a plain program's by a relative error of at most 0.03.
Values may be sent and summed in bfloat16 or wider, within the bound.
A program may use at most 128 MiB of HBM per device.

v0:
```python
import jax
import jax.numpy as jnp
from jax import lax
from jax.sharding import PartitionSpec as P

HPG = 4
EPS = 1e-06
HIGH = lax.Precision.HIGHEST


def conv_window(history, taps, amount):
    values = history.astype(jnp.float32)
    weights = taps.astype(jnp.float32)
    summed = weights[0] * values[:, 0:amount, :]
    for distance in range(1, weights.shape[0]):
        summed = summed + weights[distance] * values[:, distance : distance + amount, :]
    return jax.nn.silu(summed)


def commit_rows(history, accepted, keep):
    picked = accepted[:, None] + jnp.arange(keep, dtype=jnp.int32)[None, :]
    select = (
        picked[:, :, None] == jnp.arange(history.shape[1], dtype=jnp.int32)[None, None, :]
    ).astype(jnp.float32)
    return jnp.einsum("skl,slc->skc", select, history.astype(jnp.float32), precision=HIGH).astype(
        jnp.bfloat16
    )


def replay_state(
    state, history_x, history_b, path_dt, conv_wx, conv_wb, accepted, rate_bias, a_rate, per_group
):
    seq_count, heads, head_dim, state_dim = state.shape
    path_len = path_dt.shape[1]
    path_xs = conv_window(history_x, conv_wx, path_len).reshape(
        seq_count, path_len, heads, head_dim
    )
    path_bs = conv_window(history_b, conv_wb, path_len).reshape(
        seq_count, path_len, heads // per_group, state_dim
    )
    path_bh = jnp.repeat(path_bs, per_group, axis=2)
    path_step = jax.nn.softplus(path_dt.astype(jnp.float32) + rate_bias)
    is_live = (jnp.arange(path_len, dtype=jnp.int32)[None, :] < accepted[:, None]).astype(
        jnp.float32
    )[:, :, None]
    log_decay = path_step * a_rate * is_live
    overall = jnp.sum(log_decay, axis=1)
    tail_sum = overall[:, None, :] - jnp.cumsum(log_decay, axis=1)
    weights = is_live * jnp.exp(tail_sum) * path_step
    grown = jnp.einsum("sjh,sjhp,sjhn->shpn", weights, path_xs, path_bh, precision=HIGH)
    return jnp.exp(overall)[:, :, None, None] * state + grown


def tree_links(parents, keep):
    seq_count, prop_count = parents.shape
    front = jnp.broadcast_to(jnp.arange(-1, keep - 1, dtype=jnp.int32)[None, :], (seq_count, keep))
    parent_ids = jnp.concatenate([front, parents + keep], axis=1)
    nodes = keep + prop_count
    links = (parent_ids[:, :, None] == jnp.arange(nodes, dtype=jnp.int32)[None, None, :]).astype(
        jnp.float32
    )
    identity = jnp.eye(prop_count, dtype=jnp.float32)[None, :, :]
    ancestry = identity + links[:, keep:, keep:]
    for turn in range(prop_count.bit_length()):
        ancestry = jnp.minimum(jnp.einsum("sij,sjk->sik", ancestry, ancestry, precision=HIGH), 1.0)
    return (links, ancestry)


def tree_conv(buffer, rows, taps, links, keep):
    values = jnp.concatenate([buffer, rows], axis=1).astype(jnp.float32)
    weights = taps.astype(jnp.float32)
    last_tap = weights.shape[0] - 1
    summed = weights[last_tap] * values
    reached = values
    for distance in range(1, last_tap + 1):
        reached = jnp.einsum("sij,sjc->sic", links, reached, precision=HIGH)
        summed = summed + weights[last_tap - distance] * reached
    return jax.nn.silu(summed[:, keep:, :])


def tree_mix(
    state,
    post_x,
    post_b,
    post_c,
    rate_rows,
    z_rows,
    ancestry,
    rate_bias,
    a_rate,
    d_skip,
    gain_out,
    per_group,
):
    seq_count, prop_count, _ = post_x.shape
    heads, head_dim, state_dim = (state.shape[1], state.shape[2], state.shape[3])
    groups = heads // per_group
    x_heads = post_x.reshape(seq_count, prop_count, heads, head_dim)
    b_groups = post_b.reshape(seq_count, prop_count, groups, state_dim)
    c_groups = post_c.reshape(seq_count, prop_count, groups, state_dim)
    step_size = jax.nn.softplus(rate_rows.astype(jnp.float32) + rate_bias)
    path_decay = jnp.einsum("sij,sjh->sih", ancestry, step_size * a_rate, precision=HIGH)
    c_heads = jnp.repeat(c_groups, per_group, axis=2)
    carried = (
        jnp.einsum("sihn,shpn->sihp", c_heads, state, precision=HIGH)
        * jnp.exp(path_decay)[:, :, :, None]
    )
    scores = jnp.einsum("sign,sjgn->sgij", c_groups, b_groups, precision=HIGH)
    scores = jnp.repeat(scores, per_group, axis=1)
    decay_t = jnp.transpose(path_decay, (0, 2, 1))
    decay_gap = decay_t[:, :, :, None] - decay_t[:, :, None, :]
    is_live = ancestry[:, None, :, :] > 0.5
    mixing = jnp.where(is_live, jnp.exp(jnp.where(is_live, decay_gap, 0.0)), 0.0)
    mixing = mixing * jnp.transpose(step_size, (0, 2, 1))[:, :, None, :]
    within = jnp.einsum("shij,sjhp->sihp", scores * mixing, x_heads, precision=HIGH)
    heads_out = carried + within + d_skip[None, None, :, None] * x_heads
    heads_out = heads_out.reshape(seq_count, prop_count, heads * head_dim) * jax.nn.silu(
        z_rows.astype(jnp.float32)
    )
    grouped = heads_out.reshape(seq_count, prop_count, groups, per_group * head_dim)
    grouped = grouped * lax.rsqrt(jnp.mean(grouped * grouped, axis=-1, keepdims=True) + EPS)
    return (grouped.reshape(seq_count, prop_count, heads * head_dim) * gain_out).astype(
        jnp.bfloat16
    )


def shards(
    tokens,
    parents,
    accepted,
    state,
    conv_x,
    conv_b,
    conv_c,
    path_x,
    path_b,
    path_c,
    path_dt,
    gain_in,
    w_x,
    w_z,
    w_b,
    w_c,
    w_dt,
    dt_bias,
    a_log,
    d_skip,
    conv_wx,
    conv_wb,
    conv_wc,
    gain_out,
    w_out,
):
    seq_local = state.shape[0]
    proposals = parents.shape[1]
    heads_local = dt_bias.shape[0]
    inner_local = w_x.shape[1]
    group_cols = w_b.shape[1]
    width = gain_in.shape[0]
    keep = conv_wx.shape[0] - 1
    tp_index = lax.axis_index("tp")
    kv_index = lax.axis_index("kv")
    slab_width = tokens.shape[2]
    flat_rows = tokens.reshape(-1, slab_width).astype(jnp.float32)
    gain_part = lax.dynamic_slice_in_dim(gain_in, kv_index * slab_width, slab_width)
    scaled = (flat_rows * gain_part).astype(jnp.bfloat16)
    w_joined = jnp.concatenate([w_x, w_z, w_b, w_c], axis=1)
    joined = lax.psum_scatter(
        jnp.dot(scaled, w_joined, preferred_element_type=jnp.float32).astype(jnp.bfloat16),
        "kv",
        scatter_dimension=0,
        tiled=True,
    ).astype(jnp.float32)
    w_rate = lax.dynamic_slice(
        w_dt, (kv_index * slab_width, tp_index * heads_local), (slab_width, heads_local)
    )
    rate_term = jnp.dot(scaled, w_rate, preferred_element_type=jnp.float32)
    squares = jnp.sum(flat_rows * flat_rows, axis=1)
    rate_raw, squares = (
        lax.psum_scatter(
            rate_term.astype(jnp.bfloat16), "kv", scatter_dimension=0, tiled=True
        ).astype(jnp.float32),
        lax.psum_scatter(
            squares.astype(jnp.bfloat16), "kv", scatter_dimension=0, tiled=True
        ).astype(jnp.float32),
    )
    row_scale = lax.rsqrt(squares / width + EPS)[:, None]

    def column_part(lower, upper):
        return (
            (joined[:, lower:upper] * row_scale)
            .astype(jnp.bfloat16)
            .reshape(seq_local, proposals, upper - lower)
        )

    x_rows = column_part(0, inner_local)
    z_rows = column_part(inner_local, 2 * inner_local)
    b_rows = column_part(2 * inner_local, 2 * inner_local + group_cols)
    c_rows = column_part(2 * inner_local + group_cols, 2 * inner_local + 2 * group_cols)
    rate_rows = (
        (rate_raw * row_scale).astype(jnp.bfloat16).reshape(seq_local, proposals, heads_local)
    )
    a_rate = -jnp.exp(a_log)
    history_x = jnp.concatenate([conv_x, path_x], axis=1)
    history_b = jnp.concatenate([conv_b, path_b], axis=1)
    history_c = jnp.concatenate([conv_c, path_c], axis=1)
    new_state = replay_state(
        state, history_x, history_b, path_dt, conv_wx, conv_wb, accepted, dt_bias, a_rate, HPG
    )
    links, ancestry = tree_links(parents, keep)
    post_x = tree_conv(commit_rows(history_x, accepted, keep), x_rows, conv_wx, links, keep)
    post_b = tree_conv(commit_rows(history_b, accepted, keep), b_rows, conv_wb, links, keep)
    post_c = tree_conv(commit_rows(history_c, accepted, keep), c_rows, conv_wc, links, keep)
    gated = tree_mix(
        new_state,
        post_x,
        post_b,
        post_c,
        rate_rows,
        z_rows,
        ancestry,
        dt_bias,
        a_rate,
        d_skip,
        gain_out,
        HPG,
    )
    gated_flat = gated.reshape(-1, inner_local)
    partial_out = jnp.dot(
        gated_flat,
        lax.all_gather(w_out, "kv", axis=1, tiled=True),
        preferred_element_type=jnp.float32,
    )
    summed = lax.psum_scatter(
        partial_out.astype(jnp.bfloat16), "tp", scatter_dimension=1, tiled=True
    )
    mixed = summed.reshape(seq_local, proposals, -1)
    return (mixed, new_state)


def solution(mesh):
    return jax.shard_map(
        shards,
        mesh=mesh,
        in_specs=(
            P(None, None, "kv"),
            P("kv", None),
            P("kv"),
            P("kv", "tp", None, None),
            P("kv", None, "tp"),
            P("kv", None, "tp"),
            P("kv", None, "tp"),
            P("kv", None, "tp"),
            P("kv", None, "tp"),
            P("kv", None, "tp"),
            P("kv", None, "tp"),
            P(),
            P("kv", "tp"),
            P("kv", "tp"),
            P("kv", "tp"),
            P("kv", "tp"),
            P(),
            P("tp"),
            P("tp"),
            P("tp"),
            P(None, "tp"),
            P(None, "tp"),
            P(None, "tp"),
            P("tp"),
            P("tp", "kv"),
        ),
        out_specs=(P("kv", None, "tp"), P("kv", "tp", None, None)),
        check_vma=False,
    )
```

profile of v0, /device:TPU:0, one launch (start us, length us, event | category | flops | bytes accessed | tf_op | source)
XLA Modules:
  0.0 339.4 jit_solution(18268738023173111490)
XLA Ops:
  7.2 1.7 copy.118
  8.9 1.3 reshape.169
  10.3 0.8 dynamic_slice.6
  11.0 1.7 convolution_convert_fusion.2
  12.7 0.8 copy.153
  13.6 7.0 %convolution_convert_fusion = bf16[768,3072]{1,0:T(8,128)(2,1)} fusion(bf16[512,512]{1,0:T(8,128)(2,1)S(1)} %copy-done.19, bf16[512,512]{1,0:T(8,128)(2,1)} %param.39, bf16[512,1024]{1,0:T(8,128)(2,1)} %param.38, bf16[512,1024]{1,0:T(8,128)(2,1)} %param.37, f32[768,512]{1,0:T(8,128)} %reshape.169, f32[512]{0:T(512)S(1)} %dynamic_slice.6), kind=kOutput, calls=%fused_computation | convolution fusion | flops 2431647744 | bytes 9439232 | tf_op jit(solution)/shard_map/dot_general | solution.py:169
  25.6 23.1 %all-reduce = bf16[768]{0:T(1024)(128)(2,1)S(1)} all-reduce(bf16[768]{0:T(1024)(128)(2,1)S(1)} %convert_element_type.147), channel_id=3, replica_groups=mesh['kv'=8,'tp'=4] {'kv'}, use_global_device_ids=true, to_apply=%region_4.5.clone | all-reduce | flops 768 | bytes 3072
  50.2 10.3 %multiply_add_fusion = f32[8,16,64,128]{3,2,1,0:T(8,128)} fusion(f32[8,16,64,128]{3,2,1,0:T(8,128)} %param.28, f32[8,6,16,128]{3,1,2,0:T(8,128)S(1)} %bitcast.70, f32[8,16]{1,0:T(8,128)S(1)} %exp.57, f32[8,6,16,64]{3,2,0,1:T(8,128)S(1)} %broadcast_multiply_fusion), kind=kOutput, calls=%fused_computation.2 | convolution fusion | flops 77594624 | bytes 8978944 | tf_op jit(solution)/shard_map/sjh,sjhp,sjhn->shpn/dot_general | solution.py:50
  60.5 18.1 %reduce-scatter.10.cloned.1.call-done = bf16[96,16]{1,0:T(8,128)(2,1)} async-done(((bf16[768,16]{1,0:T(8,128)(2,1)}), bf16[96,16]{1,0:T(8,128)(2,1)}) %reduce-scatter.10.cloned.1.call-update) | async-done | bytes 3088
  78.6 0.8 copy.154
  80.2 96.8 %reduce-scatter.6.cloned.1.call-done = bf16[96,3072]{1,0:T(8,128)(2,1)} async-done(((bf16[768,3072]{1,0:T(8,128)(2,1)}), bf16[96,3072]{1,0:T(8,128)(2,1)}) %reduce-scatter.6.cloned.1.call-update) | async-done | bytes 589840 | tf_op jit(solution)/shard_map/reduce_scatter | solution.py:168
  177.0 1.2 convert_element_type.144
  180.5 1.4 multiply_bitcast_fusion
  181.9 0.8 copy.125
  184.4 0.7 divide_multiply_fusion
  185.5 1.8 fusion.33
  187.5 1.9 fusion.10
  189.5 6.8 %fusion.116 = f32[8,16,64,12]{2,3,1,0:T(8,128)S(1)} fusion(f32[8,16,64,128]{3,2,1,0:T(8,128)S(1)} %copy-done.1, f32[8,12,16,128]{3,1,2,0:T(8,128)S(1)} %bitcast.68), kind=kOutput, calls=%fused_computation.191 | convolution fusion | flops 150994944 | bytes 5373952 | tf_op jit(solution)/shard_map/sihn,shpn->sihp/dot_general | solution.py:105
  196.3 1.1 multiply_reduce_fusion.1
  198.2 105.5 %all-gather.2.cloned.1.call-done = bf16[1024,4096]{1,0:T(8,128)(2,1)} async-done(((bf16[1024,512]{1,0:T(8,128)(2,1)}), bf16[1024,4096]{1,0:T(8,128)(2,1)}) %all-gather.2.cloned.1.call-update) | async-done | bytes 8388624 | tf_op jit(solution)/shard_map/all_gather | solution.py:231
  303.7 5.8 %convolution_convert_fusion.1 = bf16[96,4096]{1,0:T(8,128)(2,1)} fusion(bf16[1024,4096]{1,0:T(8,128)(2,1)} %all-gather.2.cloned.1.call-done, f32[96,1024]{1,0:T(8,128)S(1)} %bitcast.69, f32[96,1024]{1,0:T(8,128)S(1)} %reshape.167, f32[96,1024]{1,0:T(8,128)S(1)} %get-tuple-element.15, f32[1024]{0:T(1024)S(1)} %copy-done.6), kind=kOutput, calls=%fused_computation.1 | convolution fusion | flops 806486016 | bytes 10358784 | tf_op jit(solution)/shard_map/dot_general | solution.py:229
  309.5 21.6 %reduce-scatter.8.cloned.1.call-done = bf16[96,1024]{1,0:T(8,128)(2,1)} async-done(((bf16[96,4096]{1,0:T(8,128)(2,1)}), bf16[96,1024]{1,0:T(8,128)(2,1)}) %reduce-scatter.8.cloned.1.call-update) | async-done | bytes 196624 | tf_op jit(solution)/shard_map/reduce_scatter | solution.py:234
  331.1 1.0 reshape.168
  332.1 0.8 copy.152
  (145 shorter events, 11.2 us)
Async XLA Ops:
  7.2 3.9 %copy-start = (bf16[4096,64]{0,1:T(8,128)(2,1)S(1)}, bf16[4096,64]{0,1:T(8,128)(2,1)}, u32[]{:S(2)}) copy-start(bf16[4096,64]{0,1:T(8,128)(2,1)} %param.41) | copy-start | bytes 1572868
  7.2 71.5 %reduce-scatter.10.cloned.1.call-start = ((), (), s32[]{:S(2)}) async-start(), calls=%async_computation.6 | async-start | bytes 221184
  7.2 6.4 %copy-start.19 = (bf16[512,512]{1,0:T(8,128)(2,1)S(1)}, bf16[512,512]{1,0:T(8,128)(2,1)}, u32[]{:S(2)}) copy-start(bf16[512,512]{1,0:T(8,128)(2,1)} %param.40) | copy-start | bytes 1572868
  13.6 163.4 %reduce-scatter.6.cloned.1.call-start = ((), (), s32[]{:S(2)}) async-start(), calls=%async_computation.3 | async-start | bytes 5308416 | tf_op jit(solution)/shard_map/reduce_scatter | solution.py:168
  20.6 1.6 copy-start.11
  20.6 1.7 copy-start.17
  20.7 2.0 copy-start.8
  20.7 2.0 copy-start.12
  20.7 2.3 copy-start.5
  20.7 2.3 copy-start.9
  20.7 2.5 copy-start.10
  20.7 3.0 copy-start.13
  20.8 3.2 copy-start.20
  20.8 3.2 copy-start.4
  20.8 3.2 copy-start.15
  20.8 3.6 %copy-start.21 = (u32[32]{0:T(128)S(1)}, u32[32]{0:T(128)}, u32[]{:S(2)}) copy-start(u32[32]{0:T(128)} %constant.57) | copy-start | bytes 388
  20.8 28.1 %copy-start.16 = (s32[8,12]{1,0:T(8,128)S(1)}, s32[8,12]{1,0:T(8,128)}, u32[]{:S(2)}) copy-start(s32[8,12]{1,0:T(8,128)} %param.26) | copy-start | bytes 1156
  20.8 28.1 %copy-start.14 = (bf16[4,512]{1,0:T(4,128)(2,1)S(1)}, bf16[4,512]{1,0:T(4,128)(2,1)}, u32[]{:S(2)}) copy-start(bf16[4,512]{1,0:T(4,128)(2,1)} %param.47) | copy-start | bytes 12292
  20.8 282.9 %all-gather.2.cloned.1.call-start = ((), (), s32[]{:S(2)}) async-start(), calls=%async_computation.4 | async-start | bytes 9437184 | tf_op jit(solution)/shard_map/all_gather | solution.py:231
  21.6 309.5 %reduce-scatter.8.cloned.1.call-start = ((), (), s32[]{:S(2)}) async-start(), calls=%async_computation.5 | async-start | bytes 983040 | tf_op jit(solution)/shard_map/reduce_scatter | solution.py:234
  185.3 4.1 %copy-start.3 = (f32[8,12,4,128]{3,1,2,0:T(8,128)S(1)}, f32[8,12,4,128]{3,1,2,0:T(8,128)}, u32[]{:S(2)}) copy-start(f32[8,12,4,128]{3,1,2,0:T(8,128)} %copy.125) | copy-start | bytes 589828
  185.5 4.0 %copy-start.1 = (f32[8,16,64,128]{3,2,1,0:T(8,128)S(1)}, f32[8,16,64,128]{3,2,1,0:T(8,128)}, u32[]{:S(2)}) copy-start(f32[8,16,64,128]{3,2,1,0:T(8,128)} %multiply_add_fusion) | copy-start | bytes 12582916
  189.4 6.9 %copy-start.18 = (f32[16]{0:T(128)S(1)}, f32[16]{0:T(128)}, u32[]{:S(2)}) copy-start(f32[16]{0:T(128)} %param.44) | copy-start | bytes 196
  196.3 107.4 %copy-start.6 = (f32[1024]{0:T(1024)S(1)}, f32[1024]{0:T(1024)}, u32[]{:S(2)}) copy-start(f32[1024]{0:T(1024)} %param.48) | copy-start | bytes 12292
  (2 other events, 2.7 us)
Sparse Core Ops, SparseCore 0:
  13.7 64.8 reduce-scatter.9
  82.3 94.7 reduce-scatter.5
  179.1 124.5 all-gather.1
  309.7 21.3 reduce-scatter.7
where the time goes:
time: 340 us; the launch traced here: 339 us
  waiting for transfers between devices  243 us (71%)
  matrix products  39.9 us (12%)
  blocking collectives  23.1 us (7%)
  between operations  15.3 us (4%)
  local copies, waits for them, and re-layouts  12.2 us (4%)
  other arithmetic  6.04 us (2%)
    all_gather x1, waiting for transfers between devices, shards(): lax.all_gather(w_out, 'kv', axis=1, tiled=True)  105 us
    reduce_scatter x1, waiting for transfers between devices, shards(): lax.psum_scatter(jnp.dot(scaled, w_joined, preferred_element_type=jnp.flo...  96.8 us
    unnamed x1, blocking collectives  23.1 us
    reduce_scatter x1, waiting for transfers between devices, shards(): lax.psum_scatter(partial_out.astype(jnp.bfloat16), 'tp', scatter_dimensio...  21.6 us
    unnamed x5, waiting for transfers between devices  18.9 us
    dot_general x1, matrix products, replay_state(): jnp.einsum('sjh,sjhp,sjhn->shpn', weights, path_xs, path_bh, precision=HIGH)  10.3 us
    dot_general x1, matrix products, shards(): jnp.dot(scaled, w_joined, preferred_element_type=jnp.float32)  6.99 us
    dot_general x1, matrix products, tree_mix(): jnp.einsum('sihn,shpn->sihp', c_heads, state, precision=HIGH)  6.82 us
  transfers between devices with their start and end apart: 4, of which 4 were waited for; matrix products, arithmetic and copies ran while one was open for 13% of the time, Pallas kernels for 0%

commit v1 on v0

--- a/solution.py
+++ b/solution.py
@@ -228,7 +228,15 @@
     gated_flat = gated.reshape(-1, inner_local)
     partial_out = jnp.dot(
         gated_flat,
-        lax.all_gather(w_out, "kv", axis=1, tiled=True),
+        jnp.concatenate(
+            lax.all_to_all(
+                jnp.stack(lax.psum(1, axis_name="kv") * [w_out], 0),
+                axis_name="kv",
+                split_axis=0,
+                concat_axis=0,
+            ),
+            1,
+        ),
         preferred_element_type=jnp.float32,
     )
     summed = lax.psum_scatter(

time: 340 us -> 366 us (1.076)
  blocking collectives: 23.1 us -> 149 us
  waiting for transfers between devices: 243 us -> 129 us
  starting transfers between devices: 0.16 us -> 7.53 us
  local copies, waits for them, and re-layouts: 12.2 us -> 17.7 us
    unnamed x1, blocking collectives: 23.1 us -> 149 us
    all_gather x1 -> x0, waiting for transfers between devices: 105 us -> none  [shards(): lax.all_gather(w_out, 'kv', axis=1, tiled=True)]
    unnamed x5 -> x4, waiting for transfers between devices: 18.9 us -> 7.86 us
    all_to_all x0 -> x1, starting transfers between devices: none -> 7.41 us  [shards(): lax.all_to_all(jnp.stack(lax.psum(1, axis_name='kv') * [w_out], 0), axis_...]
    another operation x0 -> x1, local copies, waits for them, and re-layouts: none -> 4.31 us  [shards(): jnp.stack(lax.psum(1, axis_name='kv') * [w_out], 0)]
  transfers between devices with their start and end apart: 4 -> 4, of which waited for: 4 -> 3; matrix products, arithmetic and copies ran while one was open for 13% -> 13% of each run, Pallas kernels for 0% -> 0%
where the time goes in v1:
time: 366 us; the launch traced here: 365 us
  blocking collectives  149 us (41%)
  waiting for transfers between devices  129 us (35%)
  matrix products  40 us (11%)
  local copies, waits for them, and re-layouts  17.7 us (5%)
  between operations  15.4 us (4%)
  starting transfers between devices  7.53 us (2%)
  other arithmetic  5.94 us (2%)
    unnamed x1, blocking collectives  149 us
    reduce_scatter x1, waiting for transfers between devices, shards(): lax.psum_scatter(jnp.dot(scaled, w_joined, preferred_element_type=jnp.flo...  98.2 us
    reduce_scatter x1, waiting for transfers between devices, shards(): lax.psum_scatter(partial_out.astype(jnp.bfloat16), 'tp', scatter_dimensio...  23 us
    dot_general x1, matrix products, replay_state(): jnp.einsum('sjh,sjhp,sjhn->shpn', weights, path_xs, path_bh, precision=HIGH)  10.3 us
    unnamed x4, waiting for transfers between devices  7.86 us
    all_to_all x1, starting transfers between devices, shards(): lax.all_to_all(jnp.stack(lax.psum(1, axis_name='kv') * [w_out], 0), axis_...  7.41 us
  transfers between devices with their start and end apart: 4, of which 3 were waited for; matrix products, arithmetic and copies ran while one was open for 13% of the time, Pallas kernels for 0%

profile of v1, /device:TPU:0, one launch (start us, length us, event | category | flops | bytes accessed | tf_op | source)
XLA Modules:
  0.0 365.1 jit_solution(323920717597913856)
XLA Ops:
  7.2 1.5 copy.154
  8.7 4.3 %stack.2 = bf16[8,1024,512]{1,2,0:T(8,128)(2,1)} broadcast(bf16[1024,512]{0,1:T(8,128)(2,1)S(1)} %copy.154), dimensions={1,2} | broadcast | bytes 9437184 | tf_op jit(solution)/shard_map/stack | solution.py:233
  13.0 7.4 %all-to-all-start = ((bf16[8,1024,512]{1,2,0:T(8,128)(2,1)}), bf16[8,1024,512]{1,2,0:T(8,128)(2,1)}, u32[]{:S(2)}, u32[]{:S(2)}) async-start(bf16[8,1024,512]{1,2,0:T(8,128)(2,1)} %stack.2), calls=%async_computation.1 | async-start | bytes 16777216 | tf_op jit(solution)/shard_map/all_to_all | solution.py:232
  21.0 1.3 reshape.179
  22.3 0.8 dynamic_slice.6
  23.1 1.7 convolution_convert_fusion.2
  24.8 0.8 copy.156
  25.7 7.1 %convolution_convert_fusion = bf16[768,3072]{1,0:T(8,128)(2,1)} fusion(bf16[512,512]{1,0:T(8,128)(2,1)} %param.40, bf16[512,512]{1,0:T(8,128)(2,1)} %param.39, bf16[512,1024]{1,0:T(8,128)(2,1)} %param.38, bf16[512,1024]{1,0:T(8,128)(2,1)} %param.37, f32[768,512]{1,0:T(8,128)} %reshape.179, f32[512]{0:T(512)S(1)} %dynamic_slice.6), kind=kOutput, calls=%fused_computation | convolution fusion | flops 2431647744 | bytes 9439232 | tf_op jit(solution)/shard_map/dot_general | solution.py:169
  37.1 149.4 %all-reduce = bf16[768]{0:T(1024)(128)(2,1)S(1)} all-reduce(bf16[768]{0:T(1024)(128)(2,1)S(1)} %convert_element_type.147), channel_id=3, replica_groups=mesh['kv'=8,'tp'=4] {'kv'}, use_global_device_ids=true, to_apply=%region_4.5.clone | all-reduce | flops 768 | bytes 3072
  188.5 10.3 %multiply_add_fusion = f32[8,16,64,128]{3,2,1,0:T(8,128)} fusion(f32[8,16,64,128]{3,2,1,0:T(8,128)} %param.28, f32[8,6,16,128]{3,1,2,0:T(8,128)S(1)} %bitcast.72, f32[8,16]{1,0:T(8,128)S(1)} %exp.57, f32[8,6,16,64]{3,2,0,1:T(8,128)S(1)} %broadcast_multiply_fusion), kind=kOutput, calls=%fused_computation.2 | convolution fusion | flops 77594624 | bytes 8978944 | tf_op jit(solution)/shard_map/sjh,sjhp,sjhn->shpn/dot_general | solution.py:50
  198.8 7.8 %reduce-scatter.10.cloned.1.call-done = bf16[96,16]{1,0:T(8,128)(2,1)} async-done(((bf16[768,16]{1,0:T(8,128)(2,1)}), bf16[96,16]{1,0:T(8,128)(2,1)}) %reduce-scatter.10.cloned.1.call-update) | async-done | bytes 3088
  206.6 0.8 copy.157
  208.2 98.2 %reduce-scatter.6.cloned.1.call-done = bf16[96,3072]{1,0:T(8,128)(2,1)} async-done(((bf16[768,3072]{1,0:T(8,128)(2,1)}), bf16[96,3072]{1,0:T(8,128)(2,1)}) %reduce-scatter.6.cloned.1.call-update) | async-done | bytes 589840 | tf_op jit(solution)/shard_map/reduce_scatter | solution.py:168
  306.4 1.2 convert_element_type.144
  307.7 1.1 reshape.181
  314.2 0.8 multiply_bitcast_fusion
  315.1 0.7 fusion.33
  315.9 1.9 fusion.10
  317.9 6.8 %fusion.116 = f32[8,16,64,12]{2,3,1,0:T(8,128)S(1)} fusion(f32[8,16,64,128]{3,2,1,0:T(8,128)S(1)} %copy-done.1, f32[8,12,16,128]{3,1,2,0:T(8,128)S(1)} %bitcast.71), kind=kOutput, calls=%fused_computation.191 | convolution fusion | flops 150994944 | bytes 5373952 | tf_op jit(solution)/shard_map/sihn,shpn->sihp/dot_general | solution.py:105
  324.8 1.1 multiply_reduce_fusion.1
  326.7 7.0 %convolution_convert_fusion.1 = bf16[96,4096]{1,0:T(8,128)(2,1)} fusion(bf16[1024,4096]{0,1:T(8,128)(2,1)} %bitcast.24, f32[96,1024]{1,0:T(8,128)S(1)} %bitcast.73, f32[96,1024]{1,0:T(8,128)S(1)} %reshape.175, f32[96,1024]{1,0:T(8,128)S(1)} %get-tuple-element.15, f32[1024]{0:T(1024)S(1)} %copy-done.22), kind=kOutput, calls=%fused_computation.1 | convolution fusion | flops 806486016 | bytes 10358784 | tf_op jit(solution)/shard_map/dot_general | solution.py:229
  333.7 23.0 %reduce-scatter.8.cloned.1.call-done = bf16[96,1024]{1,0:T(8,128)(2,1)} async-done(((bf16[96,4096]{1,0:T(8,128)(2,1)}), bf16[96,1024]{1,0:T(8,128)(2,1)}) %reduce-scatter.8.cloned.1.call-update) | async-done | bytes 196624 | tf_op jit(solution)/shard_map/reduce_scatter | solution.py:242
  356.8 1.0 reshape.178
  357.7 0.8 copy.155
  (158 shorter events, 12.9 us)
Async XLA Ops:
  7.2 15.9 %copy-start = (bf16[4096,64]{0,1:T(8,128)(2,1)S(1)}, bf16[4096,64]{0,1:T(8,128)(2,1)}, u32[]{:S(2)}) copy-start(bf16[4096,64]{0,1:T(8,128)(2,1)} %param.41) | copy-start | bytes 1572868
  13.0 7.5 %copy-start.3 = (bf16[64,12,512]{2,0,1:T(8,128)(2,1)S(1)}, bf16[64,12,512]{2,0,1:T(8,128)(2,1)}, u32[]{:S(2)}) copy-start(bf16[64,12,512]{2,0,1:T(8,128)(2,1)} %param.25) | copy-start | bytes 2359300
  13.0 313.6 %all-to-all-start = ((bf16[8,1024,512]{1,2,0:T(8,128)(2,1)}), bf16[8,1024,512]{1,2,0:T(8,128)(2,1)}, u32[]{:S(2)}, u32[]{:S(2)}) async-start(bf16[8,1024,512]{1,2,0:T(8,128)(2,1)} %stack.2), calls=%async_computation.1 | async-start | bytes 16777216 | tf_op jit(solution)/shard_map/all_to_all | solution.py:232
  20.5 186.2 %reduce-scatter.10.cloned.1.call-start = ((), (), s32[]{:S(2)}) async-start(), calls=%async_computation.6 | async-start | bytes 221184
  25.6 280.7 %reduce-scatter.6.cloned.1.call-start = ((), (), s32[]{:S(2)}) async-start(), calls=%async_computation.4 | async-start | bytes 5308416 | tf_op jit(solution)/shard_map/reduce_scatter | solution.py:168
  32.8 2.0 copy-start.14
  32.9 2.3 copy-start.26
  32.9 2.3 copy-start.4
  32.9 2.3 copy-start.16
  32.9 2.5 copy-start.9
  32.9 2.9 copy-start.27
  32.9 153.6 %copy-start.23 = (s32[8,12]{1,0:T(8,128)S(1)}, s32[8,12]{1,0:T(8,128)}, u32[]{:S(2)}) copy-start(s32[8,12]{1,0:T(8,128)} %param.26) | copy-start | bytes 1156
  32.9 153.7 %copy-start.15 = (bf16[4,512]{1,0:T(4,128)(2,1)S(1)}, bf16[4,512]{1,0:T(4,128)(2,1)}, u32[]{:S(2)}) copy-start(bf16[4,512]{1,0:T(4,128)(2,1)} %param.47) | copy-start | bytes 12292
  33.0 323.8 %reduce-scatter.8.cloned.1.call-start = ((), (), s32[]{:S(2)}) async-start(), calls=%async_computation.5 | async-start | bytes 983040 | tf_op jit(solution)/shard_map/reduce_scatter | solution.py:242
  34.9 153.1 %copy-start.12 = (f32[1,512]{1,0:T(1,128)}, f32[1,512]{1,0:T(1,128)S(1)}, u32[]{:S(2)}) copy-start(f32[1,512]{1,0:T(1,128)S(1)} %get-tuple-element.29) | copy-start | bytes 6148
  186.6 121.0 %copy-start.21 = (f32[96]{0:T(128)}, f32[96]{0:T(128)S(1)}, u32[]{:S(2)}) copy-start(f32[96]{0:T(128)S(1)} %fusion.103) | copy-start | bytes 1156
  311.2 2.9 copy-start.13
  311.2 2.9 copy-start.17
  311.2 2.9 copy-start.18
  311.3 2.9 copy-start.19
  311.3 2.9 copy-start.20
  314.2 3.7 %copy-start.1 = (f32[8,16,64,128]{3,2,1,0:T(8,128)S(1)}, f32[8,16,64,128]{3,2,1,0:T(8,128)}, u32[]{:S(2)}) copy-start(f32[8,16,64,128]{3,2,1,0:T(8,128)} %multiply_add_fusion) | copy-start | bytes 12582916
  317.8 6.9 %copy-start.2 = (f32[8,12,16,64]{3,2,1,0:T(8,128)S(1)}, f32[8,12,16,64]{3,2,1,0:T(8,128)}, u32[]{:S(2)}) copy-start(f32[8,12,16,64]{3,2,1,0:T(8,128)} %reshape.181) | copy-start | bytes 1179652
  317.8 6.9 %copy-start.25 = (f32[16]{0:T(128)S(1)}, f32[16]{0:T(128)}, u32[]{:S(2)}) copy-start(f32[16]{0:T(128)} %param.44) | copy-start | bytes 196
  (8 other events, 10.9 us)
Sparse Core Ops, SparseCore 0:
  25.8 180.8 reduce-scatter.9
  210.3 96.0 reduce-scatter.5
  333.9 22.8 reduce-scatter.7
